TPU v7x, 32 devices: a whole 2x2x4 slice. The times are simulated.
32 devices in a mesh: fs: 4 (over y, x), tp: 8 (over z, core).
Axes of the slice: x: 2, y: 2, z: 4, core: 2. Of those that a mesh axis runs over, the one named last changes fastest.
Arguments:
- tokens: bfloat16 [4096, 2048], P(('fs', 'tp')), may hold values from -6 to 6
- norm_gain: float32 [2048], replicated, may hold values from 0.1 to 1.9
- gate_weight: bfloat16 [2048, 5632], P('fs', 'tp'), may hold values from -0.125 to 0.125
- up_weight: bfloat16 [2048, 5632], P('fs', 'tp'), may hold values from -0.125 to 0.125
- down_weight: bfloat16 [5632, 2048], P('tp', 'fs'), may hold values from -0.078125 to 0.078125
Outputs:
- mixed: bfloat16 [4096, 2048], P(('fs', 'tp'))
All inputs are finite; a program needn't handle non-finite values.
Results may differ from a plain program's by a relative error of at most 0.0065.
Values may be sent and summed in bfloat16 or wider, within the bound.
A program may use at most 128 MiB of HBM per device.

v0:
```python
import functools
import math

import jax
import jax.numpy as jnp
from jax import lax
from jax.experimental import pallas as pl
from jax.experimental.pallas import tpu as pltpu

eps_floor = 0.05
MESH = pl.DeviceIdType.MESH
F32 = jnp.float32
BF16 = jnp.bfloat16


def kernel(Y, X, Z, C, cuts, tok, gain, gw, uw, dw, out, nrm, Wg, Wu, Wd, acc_g, acc_u, hid,
           sib_s, sib_r, rs_s, rs_r, part, w_local,
           w_send, w_recv, t_send, t_recv, ts_send, ts_recv, p_send, p_recv, q_send, q_recv):
    F = Y * X
    f = lax.axis_index("fs")
    t = lax.axis_index("tp")
    y, x = f // X, f % X
    z, c = t // C, t % C
    rows, D = tok.shape
    H, K = gw.shape
    N = dw.shape[1] // cuts
    tile = 2 if Z % 2 == 0 else 1

    def fs_at(j, i):
        return lax.rem(y + j, Y) * X + lax.rem(x + i, X)

    def tp_at(zz, cc):
        return zz * C + cc

    sib = lax.rem(c + 1, C)

    barrier = pltpu.get_barrier_semaphore()
    peers = [{"fs": fs_at(0, i)} for i in range(1, X)] + [{"fs": fs_at(j, 0)} for j in range(1, Y)]
    if C > 1:
        peers += [{"tp": tp_at(z, sib)}]

    def greet(peer):
        pl.semaphore_signal(barrier, inc=1, device_id=peer, device_id_type=MESH)

    for peer in peers:
        greet(peer)
    below, above = jnp.maximum(z - 1, 0), jnp.minimum(z + 1, Z - 1)
    pl.when(z > 0)(lambda: greet({"tp": tp_at(below, c)}))
    pl.when(z < Z - 1)(lambda: greet({"tp": tp_at(above, c)}))

    mats = ((gw, Wg), (uw, Wu), (dw, Wd))
    own_copies = [pltpu.make_async_copy(ref, held.at[f], w_local.at[m]) for m, (ref, held) in enumerate(mats)]
    for cp in own_copies:
        cp.start()

    pl.semaphore_wait(barrier, len(peers) + (z > 0).astype(jnp.int32) + (z < Z - 1).astype(jnp.int32))
    for cp in own_copies:
        cp.wait()

    w_copies = []

    def piece(m, h, j, i):
        held = mats[m][1].at[fs_at(j, i)]
        if m == 2 and cuts == 2:
            return held.at[:, pl.ds(h * N, N)]
        n = held.shape[0] // 2
        return held.at[pl.ds(h * n, n)]

    def w_copy(m, h, j, i, dj, di):
        k = len(w_copies)
        slot = ((j - dj) % Y) * X + (i - di) % X
        cp = pltpu.make_async_remote_copy(
            src_ref=piece(m, h, j, i), dst_ref=piece(m, h, j, i),
            send_sem=w_send.at[k], recv_sem=w_recv.at[m, h, slot],
            device_id={"fs": fs_at(dj, di)}, device_id_type=MESH)
        cp.start()
        w_copies.append(cp)

    def w_wait(m, h, j, i):
        ref = piece(m, h, j, i)
        pltpu.make_async_copy(ref, ref, w_recv.at[m, h, j * X + i]).wait()

    def phase_one(ms):
        for m in ms:
            for i in range(1, X):
                w_copy(m, 0, 0, 0, 0, i)
            for j in range(1, Y):
                w_copy(m, 1, 0, 0, j, 0)

    def phase_own(ms):
        for m in ms:
            for i in range(1, X):
                w_copy(m, 1, 0, 0, 0, i)
            for j in range(1, Y):
                w_copy(m, 0, 0, 0, j, 0)

    def phase_relay(ms):
        for m in ms:
            for i in range(1, X):
                w_wait(m, 0, 0, i)
                for j in range(1, Y):
                    w_copy(m, 0, 0, i, j, 0)
            for j in range(1, Y):
                w_wait(m, 1, j, 0)
                for i in range(1, X):
                    w_copy(m, 1, j, 0, 0, i)

    def wait_cross(ms):
        for m in ms:
            for i in range(1, X):
                w_wait(m, 1, 0, i)
            for j in range(1, Y):
                w_wait(m, 0, j, 0)

    def wait_diag(ms):
        for m in ms:
            for j in range(1, Y):
                for i in range(1, X):
                    w_wait(m, 0, j, i)
                    w_wait(m, 1, j, i)

    def tok_chain(direction, s):
        src = z - s if direction == 0 else z + s
        dst = z + 1 if direction == 0 else z - 1
        ok = jnp.logical_and(src >= 0, dst < Z) if direction == 0 else jnp.logical_and(src < Z, dst >= 0)
        src, dst = jnp.clip(src, 0, Z - 1), jnp.clip(dst, 0, Z - 1)
        cp = pltpu.make_async_remote_copy(
            src_ref=nrm.at[c, src], dst_ref=nrm.at[c, src],
            send_sem=t_send.at[direction, s], recv_sem=t_recv.at[direction, s],
            device_id={"tp": tp_at(dst, c)}, device_id_type=MESH)
        return cp, ok

    def tok_sib(zz):
        return pltpu.make_async_remote_copy(
            src_ref=nrm.at[c, zz], dst_ref=nrm.at[c, zz],
            send_sem=ts_send.at[zz], recv_sem=ts_recv.at[zz],
            device_id={"tp": tp_at(z, sib)}, device_id_type=MESH)

    def tok_start(s):
        for direction in range(2):
            cp, ok = tok_chain(direction, s)
            pl.when(ok)(cp.start)

    def tok_arrive(s):
        for direction in range(2):
            src = z - s if direction == 0 else z + s
            there = src >= 0 if direction == 0 else src < Z
            src = jnp.clip(src, 0, Z - 1)

            @pl.when(there)
            def _():
                pltpu.make_async_copy(nrm.at[c, src], nrm.at[c, src], t_recv.at[direction, s - 1]).wait()
                if C > 1:
                    tok_sib(src).start()

            if s < Z - 1:
                cp, ok = tok_chain(direction, s)
                pl.when(ok)(cp.start)

    phase_one((0, 1))
    values = tok[...].astype(F32)
    factor = lax.rsqrt(jnp.mean(values * values, axis=-1, keepdims=True) + eps_floor)
    nrm[c, z] = (values * factor * gain[...]).astype(BF16)
    tok_start(0)
    if C > 1:
        tok_sib(z).start()
    phase_own((0, 1))
    if Z > 1:
        tok_arrive(1)
    phase_relay((0, 1))
    for s in range(2, Z):
        tok_arrive(s)
    wait_cross((0, 1))
    phase_one((2,))
    phase_own((2,))
    if C > 1:
        for zz in range(Z):
            ref = nrm.at[sib, zz]
            pltpu.make_async_copy(ref, ref, ts_recv.at[zz]).wait()

    near = [(0, 0)] + [(0, i) for i in range(1, X)] + [(j, 0) for j in range(1, Y)]
    far = [(j, i) for j in range(1, Y) for i in range(1, X)]
    mrows = tile * rows
    per_core = Z // tile

    def product(n, held, group):
        cc, zt = n // per_core, n % per_core
        total = None
        for j, i in group:
            o = fs_at(j, i)
            a = nrm[cc, pl.ds(zt * tile, tile), :, pl.ds(pl.multiple_of(o * K, K), K)].reshape(mrows, K)
            p = lax.dot_general(a, held[o], (((1,), (1,)), ((), ())), preferred_element_type=F32)
            total = p if total is None else total + p
        return total

    @pl.loop(0, C * per_core)
    def _(n):
        acc_g[n] = product(n, Wg, near)
        acc_u[n] = product(n, Wu, near)

    wait_diag((0,))

    @pl.loop(0, C * per_core)
    def _(n):
        g = acc_g[n]
        if far:
            g = g + product(n, Wg, far)
        acc_g[n] = jax.nn.silu(g)

    wait_diag((1,))

    @pl.loop(0, C * per_core)
    def _(n):
        u = acc_u[n]
        if far:
            u = u + product(n, Wu, far)
        hid[n // per_core, pl.ds((n % per_core) * tile, tile)] = (acc_g[n] * u).astype(BF16).reshape(tile, rows, H)

    sib_copies = []

    def sum_copy(q, direction, d):
        to = above if direction == 0 else below
        return pltpu.make_async_remote_copy(
            src_ref=rs_s.at[q, d], dst_ref=rs_r.at[q, direction, d],
            send_sem=q_send.at[q, d], recv_sem=q_recv.at[q, direction, d],
            device_id={"tp": tp_at(to, c)}, device_id_type=MESH)

    def sum_wait(q, direction, d):
        ref = rs_r.at[q, direction, d]
        pltpu.make_async_copy(ref, ref, q_recv.at[q, direction, d]).wait()

    units = []

    def down(new):
        qs = list(range(len(units), len(units) + len(new)))
        units.extend(new)

        def weight(q):
            j, i, h = units[q]
            return Wd[fs_at(j, i), :, h * N:(h + 1) * N]

        copies = []
        if C > 1:
            for q in qs:
                sib_s[q] = jnp.dot(hid[sib].reshape(Z * rows, H), weight(q),
                                   preferred_element_type=F32).astype(BF16).reshape(Z, rows, N)
                cp = pltpu.make_async_remote_copy(
                    src_ref=sib_s.at[q], dst_ref=sib_r.at[q], send_sem=p_send.at[q], recv_sem=p_recv.at[q],
                    device_id={"tp": tp_at(z, sib)}, device_id_type=MESH)
                cp.start()
                copies.append(cp)
        for q in qs:
            part[q] = jnp.dot(hid[c].reshape(Z * rows, H), weight(q),
                              preferred_element_type=F32).reshape(Z, rows, N)
        for q, cp in zip(qs, copies):
            cp.wait_recv()

            @pl.loop(0, Z)
            def _(d):
                part[q, d] = part[q, d] + sib_r[q, d].astype(F32)
        sib_copies.extend(copies)

        for direction, first, order in ((0, z == 0, range(Z - 1, 0, -1)), (1, z == Z - 1, range(Z - 1))):
            @pl.when(first)
            def _():
                for d in order:
                    for q in qs:
                        rs_s[q, d] = part[q, d].astype(BF16)
                        sum_copy(q, direction, d).start()
        return qs

    low = 2 * z < Z

    def sum_step(q, direction, d, ok):
        @pl.when(ok)
        def _():
            sum_wait(q, direction, d)
            rs_s[q, d] = (part[q, d] + rs_r[q, direction, d].astype(F32)).astype(BF16)
            sum_copy(q, direction, d).start()

    def sum_near(qs):
        for d in range(Z - 1, 0, -1):
            for q in qs:
                sum_step(q, 0, d, jnp.logical_and(jnp.logical_and(z > 0, z < d), low))
        for d in range(Z - 1):
            for q in qs:
                sum_step(q, 1, d, jnp.logical_and(jnp.logical_and(z < Z - 1, z > d), jnp.logical_not(low)))

    def sum_far(qs):
        for d in range(Z - 1, 0, -1):
            for q in qs:
                sum_step(q, 0, d, jnp.logical_and(z < d, jnp.logical_not(low)))
        for d in range(Z - 1):
            for q in qs:
                sum_step(q, 1, d, jnp.logical_and(z > d, low))

    def sum_end(q):
        j, i, h = units[q]
        for direction, there in ((0, z > 0), (1, z < Z - 1)):
            @pl.when(there)
            def _():
                sum_wait(q, direction, z)
                part[q, z] = part[q, z] + rs_r[q, direction, z].astype(F32)

        out[:, pl.ds(pl.multiple_of((fs_at(j, i) * cuts + h) * N, N), N)] = part[q, z].astype(BF16)

    in_row = [(0, i) for i in range(1, X)]
    in_col = [(j, 0) for j in range(1, Y)]
    both = range(cuts)
    early = [(j, i, 0) for j, i in in_row] + [(j, i, 1) for j, i in in_col] if cuts == 2 else []
    mid = [(j, i, h) for h in both for j, i in in_row + in_col if (j, i, h) not in early]
    qa = [q for h in both for q in down([(0, 0, h)])]
    phase_relay((2,))
    qb = down(early)
    sum_near(qa)
    wait_cross((2,))
    qc = down(mid)
    sum_near(qb)
    sum_far(qa)
    wait_diag((2,))
    qd = down([(j, i, h) for j, i in far for h in both])
    sum_near(qc)
    sum_far(qb)
    for q in qa + qb:
        sum_end(q)
    sum_far(qc)
    sum_near(qd)
    for q in qc:
        sum_end(q)
    sum_far(qd)
    for q in qd:
        sum_end(q)

    for cp in w_copies:
        cp.wait_send()
    for s in range(Z - 1):
        for direction in range(2):
            cp, ok = tok_chain(direction, s)
            pl.when(ok)(cp.wait_send)
    if C > 1:
        for zz in range(Z):
            tok_sib(zz).wait_send()
        for cp in sib_copies:
            cp.wait_send()
    for q in range(len(units)):
        for d in range(Z):
            pl.when(z != d)(sum_copy(q, 0, d).wait_send)


def local(sizes, tokens, norm_gain, gate_weight, up_weight, down_weight):
    Y, X, Z, C = sizes
    F = Y * X
    rows, D = tokens.shape
    gate_weight, up_weight = gate_weight.T, up_weight.T
    H, K = gate_weight.shape
    cuts = 2 if down_weight.shape[1] % 256 == 0 else 1
    N = down_weight.shape[1] // cuts
    U = F * cuts
    tile = 2 if Z % 2 == 0 else 1
    n_w = 3 * ((X - 1) + (Y - 1) * X + (Y - 1) + (X - 1) * Y)
    vmem = pl.BlockSpec(memory_space=pltpu.VMEM)
    dma = pltpu.SemaphoreType.DMA
    hbm = pl.BlockSpec(memory_space=pl.ANY)
    return pl.pallas_call(
        functools.partial(kernel, Y, X, Z, C, cuts),
        out_shape=pltpu.VMEM((rows, D), BF16),
        in_specs=[vmem] * 2 + [hbm] * 3,
        out_specs=vmem,
        scratch_shapes=[
            pltpu.VMEM((C, Z, rows, D), BF16),
            pltpu.VMEM((F, H, K), BF16),
            pltpu.VMEM((F, H, K), BF16),
            pltpu.VMEM((F, H, N * cuts), BF16),
            pltpu.VMEM((C * Z // tile, tile * rows, H), F32),
            pltpu.VMEM((C * Z // tile, tile * rows, H), F32),
            pltpu.VMEM((C, Z, rows, H), BF16),
            pltpu.VMEM((U, Z, rows, N), BF16),
            pltpu.VMEM((U, Z, rows, N), BF16),
            pltpu.VMEM((U, Z, rows, N), BF16),
            pltpu.VMEM((U, 2, Z, rows, N), BF16),
            pltpu.VMEM((U, Z, rows, N), F32),
            dma((3,)),
            dma((max(n_w, 1),)), dma((3, 2, F)),
            dma((2, Z)), dma((2, Z)), dma((Z,)), dma((Z,)),
            dma((U,)), dma((U,)), dma((U, Z)), dma((U, 2, Z)),
        ],
        compiler_params=pltpu.CompilerParams(
            collective_id=0, has_side_effects=True, vmem_limit_bytes=60 * 1024 * 1024),
    )(tokens, norm_gain.reshape(1, D), gate_weight, up_weight, down_weight)


def solution(mesh):
    fs, tp = mesh.shape["fs"], mesh.shape["tp"]
    X = max(n for n in range(1, math.isqrt(fs) + 1) if fs % n == 0)
    C = 2 if tp % 2 == 0 else 1
    from jax.sharding import PartitionSpec as P
    return jax.shard_map(
        functools.partial(local, (fs // X, X, tp // C, C)),
        mesh=mesh,
        in_specs=(P(("fs", "tp"), None), P(), P("fs", "tp"), P("fs", "tp"), P("tp", "fs")),
        out_specs=P(("fs", "tp"), None),
        check_vma=False,
    )
```

profile of v0, /device:TPU:0, one launch (start us, length us, event | category | flops | bytes accessed | tf_op | source)
XLA Modules:
  0.0 98.2 jit_solution(3568475256546775424)
XLA Ops:
  0.0 97.4 %shard_map.55 = bf16[128,2048]{1,0:T(8,128)(2,1)S(1)} custom-call(bf16[128,2048]{1,0:T(8,128)(2,1)} %tok.1, f32[1,2048]{1,0:T(1,128)} %bitcast.5, bf16[704,512]{1,0:T(8,128)(2,1)} %bitcast.3, bf16[704,512]{1,0:T(8,128)(2,1)} %bitcast.4, bf16[704,512]{1,0:T(8,128)(2,1)} %dw.1), custom_call_target="tpu_custom_call" | custom-call | tf_op jit(solution)/shard_map/pallas_call | solution.py:364
  97.4 0.8 copy.7
where the time goes:
time: 98.4 us; the launch traced here: 98.2 us
  Pallas kernels  97.4 us (99%)
    pallas_call x1, Pallas kernels, local(): pl.pallas_call(functools.partial(kernel, Y, X, Z, C, cuts), out_shape=plt...  97.4 us

commit v1 on v0

--- a/solution.py
+++ b/solution.py
@@ -14,7 +14,7 @@
 
 
 def kernel(Y, X, Z, C, cuts, tok, gain, gw, uw, dw, out, nrm, Wg, Wu, Wd, acc_g, acc_u, hid,
-           sib_s, sib_r, rs_s, rs_r, part, w_local,
+           sib_s, sib_r, rs_s, rs_r, part, tok_v, gain_v, w_local,
            w_send, w_recv, t_send, t_recv, ts_send, ts_recv, p_send, p_recv, q_send, q_recv):
     F = Y * X
     f = lax.axis_index("fs")
@@ -50,14 +50,13 @@
 
     mats = ((gw, Wg), (uw, Wu), (dw, Wd))
     own_copies = [pltpu.make_async_copy(ref, held.at[f], w_local.at[m]) for m, (ref, held) in enumerate(mats)]
+    own_copies += [pltpu.make_async_copy(tok, tok_v, w_local.at[3]), pltpu.make_async_copy(gain, gain_v, w_local.at[4])]
     for cp in own_copies:
         cp.start()
 
     pl.semaphore_wait(barrier, len(peers) + (z > 0).astype(jnp.int32) + (z < Z - 1).astype(jnp.int32))
     for cp in own_copies:
         cp.wait()
-
-    w_copies = []
 
     def piece(m, h, j, i):
         held = mats[m][1].at[fs_at(j, i)]
@@ -67,14 +66,12 @@
         return held.at[pl.ds(h * n, n)]
 
     def w_copy(m, h, j, i, dj, di):
-        k = len(w_copies)
         slot = ((j - dj) % Y) * X + (i - di) % X
         cp = pltpu.make_async_remote_copy(
             src_ref=piece(m, h, j, i), dst_ref=piece(m, h, j, i),
-            send_sem=w_send.at[k], recv_sem=w_recv.at[m, h, slot],
+            send_sem=w_send.at[m], recv_sem=w_recv.at[m, h, slot],
             device_id={"fs": fs_at(dj, di)}, device_id_type=MESH)
         cp.start()
-        w_copies.append(cp)
 
     def w_wait(m, h, j, i):
         ref = piece(m, h, j, i)
@@ -133,7 +130,7 @@
     def tok_sib(zz):
         return pltpu.make_async_remote_copy(
             src_ref=nrm.at[c, zz], dst_ref=nrm.at[c, zz],
-            send_sem=ts_send.at[zz], recv_sem=ts_recv.at[zz],
+            send_sem=ts_send, recv_sem=ts_recv.at[zz],
             device_id={"tp": tp_at(z, sib)}, device_id_type=MESH)
 
     def tok_start(s):
@@ -158,9 +155,9 @@
                 pl.when(ok)(cp.start)
 
     phase_one((0, 1))
-    values = tok[...].astype(F32)
+    values = tok_v[...].astype(F32)
     factor = lax.rsqrt(jnp.mean(values * values, axis=-1, keepdims=True) + eps_floor)
-    nrm[c, z] = (values * factor * gain[...]).astype(BF16)
+    nrm[c, z] = (values * factor * gain_v[...]).astype(BF16)
     tok_start(0)
     if C > 1:
         tok_sib(z).start()
@@ -216,18 +213,19 @@
             u = u + product(n, Wu, far)
         hid[n // per_core, pl.ds((n % per_core) * tile, tile)] = (acc_g[n] * u).astype(BF16).reshape(tile, rows, H)
 
-    sib_copies = []
+    def sum_slot(direction, d, at):
+        return d if direction == 0 else jnp.where(at == d, Z, d)
 
     def sum_copy(q, direction, d):
         to = above if direction == 0 else below
         return pltpu.make_async_remote_copy(
             src_ref=rs_s.at[q, d], dst_ref=rs_r.at[q, direction, d],
-            send_sem=q_send.at[q, d], recv_sem=q_recv.at[q, direction, d],
+            send_sem=q_send, recv_sem=q_recv.at[q, sum_slot(direction, d, to)],
             device_id={"tp": tp_at(to, c)}, device_id_type=MESH)
 
     def sum_wait(q, direction, d):
         ref = rs_r.at[q, direction, d]
-        pltpu.make_async_copy(ref, ref, q_recv.at[q, direction, d]).wait()
+        pltpu.make_async_copy(ref, ref, q_recv.at[q, sum_slot(direction, d, z)]).wait()
 
     units = []
 
@@ -245,7 +243,7 @@
                 sib_s[q] = jnp.dot(hid[sib].reshape(Z * rows, H), weight(q),
                                    preferred_element_type=F32).astype(BF16).reshape(Z, rows, N)
                 cp = pltpu.make_async_remote_copy(
-                    src_ref=sib_s.at[q], dst_ref=sib_r.at[q], send_sem=p_send.at[q], recv_sem=p_recv.at[q],
+                    src_ref=sib_s.at[q], dst_ref=sib_r.at[q], send_sem=p_send, recv_sem=p_recv.at[q],
                     device_id={"tp": tp_at(z, sib)}, device_id_type=MESH)
                 cp.start()
                 copies.append(cp)
@@ -258,7 +256,6 @@
             @pl.loop(0, Z)
             def _(d):
                 part[q, d] = part[q, d] + sib_r[q, d].astype(F32)
-        sib_copies.extend(copies)
 
         for direction, first, order in ((0, z == 0, range(Z - 1, 0, -1)), (1, z == Z - 1, range(Z - 1))):
             @pl.when(first)
@@ -331,20 +328,21 @@
     for q in qd:
         sum_end(q)
 
-    for cp in w_copies:
-        cp.wait_send()
+    def sent(ref, sem):
+        pltpu.make_async_copy(ref, ref, sem).wait()
+
+    if F > 1:
+        for m in range(3):
+            sent(mats[m][1].at[pl.ds(0, F - 1)], w_send.at[m])
     for s in range(Z - 1):
         for direction in range(2):
             cp, ok = tok_chain(direction, s)
             pl.when(ok)(cp.wait_send)
     if C > 1:
-        for zz in range(Z):
-            tok_sib(zz).wait_send()
-        for cp in sib_copies:
-            cp.wait_send()
-    for q in range(len(units)):
-        for d in range(Z):
-            pl.when(z != d)(sum_copy(q, 0, d).wait_send)
+        sent(nrm.at[c], ts_send)
+        sent(sib_s, p_send)
+    if Z > 1:
+        sent(rs_s.at[:, pl.ds(0, Z - 1)], q_send)
 
 
 def local(sizes, tokens, norm_gain, gate_weight, up_weight, down_weight):
@@ -357,14 +355,13 @@
     N = down_weight.shape[1] // cuts
     U = F * cuts
     tile = 2 if Z % 2 == 0 else 1
-    n_w = 3 * ((X - 1) + (Y - 1) * X + (Y - 1) + (X - 1) * Y)
     vmem = pl.BlockSpec(memory_space=pltpu.VMEM)
     dma = pltpu.SemaphoreType.DMA
     hbm = pl.BlockSpec(memory_space=pl.ANY)
     return pl.pallas_call(
         functools.partial(kernel, Y, X, Z, C, cuts),
         out_shape=pltpu.VMEM((rows, D), BF16),
-        in_specs=[vmem] * 2 + [hbm] * 3,
+        in_specs=[hbm] * 5,
         out_specs=vmem,
         scratch_shapes=[
             pltpu.VMEM((C, Z, rows, D), BF16),
@@ -379,10 +376,12 @@
             pltpu.VMEM((U, Z, rows, N), BF16),
             pltpu.VMEM((U, 2, Z, rows, N), BF16),
             pltpu.VMEM((U, Z, rows, N), F32),
-            dma((3,)),
-            dma((max(n_w, 1),)), dma((3, 2, F)),
-            dma((2, Z)), dma((2, Z)), dma((Z,)), dma((Z,)),
-            dma((U,)), dma((U,)), dma((U, Z)), dma((U, 2, Z)),
+            pltpu.VMEM((rows, D), BF16),
+            pltpu.VMEM((1, D), F32),
+            dma((5,)),
+            dma((3,)), dma((3, 2, F)),
+            dma((2, max(Z - 1, 1))), dma((2, max(Z - 1, 1))), dma, dma((Z,)),
+            dma, dma((U,)), dma, dma((U, Z + 1)),
         ],
         compiler_params=pltpu.CompilerParams(
             collective_id=0, has_side_effects=True, vmem_limit_bytes=60 * 1024 * 1024),

time: 98.4 us -> 96.6 us (0.982)
  Pallas kernels: 97.4 us -> 95.7 us
    pallas_call x1, Pallas kernels: 97.4 us -> 95.7 us  [local(): pl.pallas_call(functools.partial(kernel, Y, X, Z, C, cuts), out_shape=plt...]
where the time goes in v1:
time: 96.6 us; the launch traced here: 96.5 us
  Pallas kernels  95.7 us (99%)
    pallas_call x1, Pallas kernels, local(): pl.pallas_call(functools.partial(kernel, Y, X, Z, C, cuts), out_shape=plt...  95.7 us

profile of v1, /device:TPU:0, one launch (start us, length us, event | category | flops | bytes accessed | tf_op | source)
XLA Modules:
  0.0 96.5 jit_solution(8413180981711110138)
XLA Ops:
  0.0 95.7 %shard_map.55 = bf16[128,2048]{1,0:T(8,128)(2,1)S(1)} custom-call(bf16[128,2048]{1,0:T(8,128)(2,1)} %tok.1, f32[1,2048]{1,0:T(1,128)} %bitcast.5, bf16[704,512]{1,0:T(8,128)(2,1)} %bitcast.3, bf16[704,512]{1,0:T(8,128)(2,1)} %bitcast.4, bf16[704,512]{1,0:T(8,128)(2,1)} %dw.1), custom_call_target="tpu_custom_call" | custom-call | tf_op jit(solution)/shard_map/pallas_call | solution.py:361
  95.7 0.8 copy.7

commit v2 on v1

--- a/solution.py
+++ b/solution.py
@@ -229,7 +229,37 @@
 
     units = []
 
-    def down(new):
+    def add_sib(q, d):
+        if C > 1:
+            part[q, d] = part[q, d] + sib_r[q, d].astype(F32)
+
+    def open_sum(qs, direction, order):
+        for d in order:
+            for q in qs:
+                total = part[q, d]
+                if C > 1:
+                    total = total + sib_r[q, d].astype(F32)
+                rs_s[q, d] = total.astype(BF16)
+                sum_copy(q, direction, d).start()
+
+    def settle(qs, hold, held):
+        def ends(direction, order):
+            open_sum(qs, direction, order[:-1])
+            if not hold:
+                open_sum(held + qs, direction, order[-1:])
+
+        if Z > 1:
+            pl.when(z == 0)(lambda: ends(0, list(range(Z - 1, 0, -1))))
+            pl.when(z == Z - 1)(lambda: ends(1, list(range(Z - 1))))
+
+        @pl.loop(0, Z)
+        def _(d):
+            @pl.when(jnp.logical_or(d == z, jnp.logical_and(z > 0, z < Z - 1)))
+            def _():
+                for q in qs:
+                    add_sib(q, d)
+
+    def down(new, apart=False, hold=False, held=()):
         qs = list(range(len(units), len(units) + len(new)))
         units.extend(new)
 
@@ -247,23 +277,15 @@
                     device_id={"tp": tp_at(z, sib)}, device_id_type=MESH)
                 cp.start()
                 copies.append(cp)
-        for q in qs:
+        for k, q in enumerate(qs):
             part[q] = jnp.dot(hid[c].reshape(Z * rows, H), weight(q),
                               preferred_element_type=F32).reshape(Z, rows, N)
-        for q, cp in zip(qs, copies):
-            cp.wait_recv()
-
-            @pl.loop(0, Z)
-            def _(d):
-                part[q, d] = part[q, d] + sib_r[q, d].astype(F32)
-
-        for direction, first, order in ((0, z == 0, range(Z - 1, 0, -1)), (1, z == Z - 1, range(Z - 1))):
-            @pl.when(first)
-            def _():
-                for d in order:
-                    for q in qs:
-                        rs_s[q, d] = part[q, d].astype(BF16)
-                        sum_copy(q, direction, d).start()
+            if C > 1:
+                copies[k].wait_recv()
+            if apart:
+                settle([q], hold, [])
+        if not apart:
+            settle(qs, hold, list(held))
         return qs
 
     low = 2 * z < Z
@@ -275,21 +297,43 @@
             rs_s[q, d] = (part[q, d] + rs_r[q, direction, d].astype(F32)).astype(BF16)
             sum_copy(q, direction, d).start()
 
-    def sum_near(qs):
-        for d in range(Z - 1, 0, -1):
+    def near_low(q, k):
+        d = Z - 1 - k
+        sum_step(q, 0, d, jnp.logical_and(jnp.logical_and(z > 0, z < d), low))
+
+    def near_high(q, k):
+        sum_step(q, 1, k, jnp.logical_and(jnp.logical_and(z < Z - 1, z > k), jnp.logical_not(low)))
+
+    def far_low(q, k):
+        sum_step(q, 1, k, jnp.logical_and(z > k, low))
+
+    def far_high(q, k):
+        d = Z - 1 - k
+        sum_step(q, 0, d, jnp.logical_and(z < d, jnp.logical_not(low)))
+
+    hops = range(Z - 1)
+
+    def sum_near(qs, ks=hops):
+        for k in ks:
             for q in qs:
-                sum_step(q, 0, d, jnp.logical_and(jnp.logical_and(z > 0, z < d), low))
-        for d in range(Z - 1):
+                near_low(q, k)
+                near_high(q, k)
+
+    def sum_far(qs):
+        for k in hops:
             for q in qs:
-                sum_step(q, 1, d, jnp.logical_and(jnp.logical_and(z < Z - 1, z > d), jnp.logical_not(low)))
-
-    def sum_far(qs):
-        for d in range(Z - 1, 0, -1):
+                far_low(q, k)
+                far_high(q, k)
+
+    def sum_last(qs):
+        for k in hops:
             for q in qs:
-                sum_step(q, 0, d, jnp.logical_and(z < d, jnp.logical_not(low)))
-        for d in range(Z - 1):
-            for q in qs:
-                sum_step(q, 1, d, jnp.logical_and(z > d, low))
+                if k + 1 < Z - 1:
+                    near_low(q, k + 1)
+                far_low(q, k)
+                far_high(q, k)
+                if k + 1 < Z - 1:
+                    near_high(q, k + 1)
 
     def sum_end(q):
         j, i, h = units[q]
@@ -306,26 +350,24 @@
     both = range(cuts)
     early = [(j, i, 0) for j, i in in_row] + [(j, i, 1) for j, i in in_col] if cuts == 2 else []
     mid = [(j, i, h) for h in both for j, i in in_row + in_col if (j, i, h) not in early]
-    qa = [q for h in both for q in down([(0, 0, h)])]
+    qa = down([(0, 0, h) for h in both], True)
     phase_relay((2,))
     qb = down(early)
     sum_near(qa)
     wait_cross((2,))
-    qc = down(mid)
+    qc = down(mid, hold=True)
     sum_near(qb)
     sum_far(qa)
     wait_diag((2,))
-    qd = down([(j, i, h) for j, i in far for h in both])
+    qd = down([(j, i, h) for j, i in far for h in both], held=qc)
     sum_near(qc)
     sum_far(qb)
     for q in qa + qb:
         sum_end(q)
     sum_far(qc)
-    sum_near(qd)
-    for q in qc:
-        sum_end(q)
-    sum_far(qd)
-    for q in qd:
+    sum_near(qd, range(min(1, Z - 1)))
+    sum_last(qd)
+    for q in qc + qd:
         sum_end(q)
 
     def sent(ref, sem):

time: 96.6 us -> 94.5 us (0.978)
  Pallas kernels: 95.7 us -> 93.6 us
    pallas_call x1, Pallas kernels: 95.7 us -> 93.6 us  [local(): pl.pallas_call(functools.partial(kernel, Y, X, Z, C, cuts), out_shape=plt...]
where the time goes in v2:
time: 94.5 us; the launch traced here: 94.4 us
  Pallas kernels  93.6 us (99%)
    pallas_call x1, Pallas kernels, local(): pl.pallas_call(functools.partial(kernel, Y, X, Z, C, cuts), out_shape=plt...  93.6 us

profile of v2, /device:TPU:0, one launch (start us, length us, event | category | flops | bytes accessed | tf_op | source)
XLA Modules:
  0.0 94.4 jit_solution(4606280918679663531)
XLA Ops:
  0.0 93.6 %shard_map.55 = bf16[128,2048]{1,0:T(8,128)(2,1)S(1)} custom-call(bf16[128,2048]{1,0:T(8,128)(2,1)} %tok.1, f32[1,2048]{1,0:T(1,128)} %bitcast.5, bf16[704,512]{1,0:T(8,128)(2,1)} %bitcast.3, bf16[704,512]{1,0:T(8,128)(2,1)} %bitcast.4, bf16[704,512]{1,0:T(8,128)(2,1)} %dw.1), custom_call_target="tpu_custom_call" | custom-call | tf_op jit(solution)/shard_map/pallas_call | solution.py:403
  93.6 0.8 copy.7

commit v3 on v2

--- a/solution.py
+++ b/solution.py
@@ -13,9 +13,9 @@
 BF16 = jnp.bfloat16
 
 
-def kernel(Y, X, Z, C, cuts, tok, gain, gw, uw, dw, out, nrm, Wg, Wu, Wd, acc_g, acc_u, hid,
+def kernel(Y, X, Z, C, cuts, R, tok, gain, gw, uw, dw, out, nrm, Wg, Wu, Wd, over, acc_g, acc_u, hid,
            sib_s, sib_r, rs_s, rs_r, part, tok_v, gain_v, w_local,
-           w_send, w_recv, t_send, t_recv, ts_send, ts_recv, p_send, p_recv, q_send, q_recv):
+           w_send, w_recv, over_recv, t_send, t_recv, ts_send, ts_recv, p_send, p_recv, q_send, q_recv):
     F = Y * X
     f = lax.axis_index("fs")
     t = lax.axis_index("tp")
@@ -25,6 +25,12 @@
     H, K = gw.shape
     N = dw.shape[1] // cuts
     tile = 2 if Z % 2 == 0 else 1
+    n0 = H // 2 - R
+    strips = 2 if rows % 32 == 0 else 1
+    strip = rows // strips
+    ups = (1, 3) if R else (1,)
+    edge = jnp.logical_or(z == 0, z == Z - 1)
+    inner = jnp.logical_or(z == 1, z == Z - 2)
 
     def fs_at(j, i):
         return lax.rem(y + j, Y) * X + lax.rem(x + i, X)
@@ -59,23 +65,30 @@
         cp.wait()
 
     def piece(m, h, j, i):
-        held = mats[m][1].at[fs_at(j, i)]
-        if m == 2 and cuts == 2:
-            return held.at[:, pl.ds(h * N, N)]
-        n = held.shape[0] // 2
-        return held.at[pl.ds(h * n, n)]
+        o = fs_at(j, i)
+        if m == 0:
+            return Wg.at[o, pl.ds(h * (H // 2), H // 2)]
+        if m == 1:
+            return Wu.at[o, pl.ds(h * n0, n0)]
+        if m == 3:
+            return Wu.at[o, pl.ds(2 * n0 + h * R, R)]
+        if m == 4:
+            return over.at[o, pl.ds(h * R, R)]
+        if cuts == 2:
+            return Wd.at[o, :, pl.ds(h * N, N)]
+        return Wd.at[o, pl.ds(h * (H // 2), H // 2)]
 
     def w_copy(m, h, j, i, dj, di):
         slot = ((j - dj) % Y) * X + (i - di) % X
         cp = pltpu.make_async_remote_copy(
             src_ref=piece(m, h, j, i), dst_ref=piece(m, h, j, i),
-            send_sem=w_send.at[m], recv_sem=w_recv.at[m, h, slot],
+            send_sem=w_send.at[m], recv_sem=w_recv.at[m, h, slot - 1],
             device_id={"fs": fs_at(dj, di)}, device_id_type=MESH)
         cp.start()
 
     def w_wait(m, h, j, i):
         ref = piece(m, h, j, i)
-        pltpu.make_async_copy(ref, ref, w_recv.at[m, h, j * X + i]).wait()
+        pltpu.make_async_copy(ref, ref, w_recv.at[m, h, j * X + i - 1]).wait()
 
     def phase_one(ms):
         for m in ms:
@@ -116,29 +129,43 @@
                     w_wait(m, 0, j, i)
                     w_wait(m, 1, j, i)
 
-    def tok_chain(direction, s):
+    def over_in():
+        o = fs_at(0, 0)
+        to = jnp.where(z == 0, 1, Z - 2)
+        return pltpu.make_async_remote_copy(
+            src_ref=Wu.at[o, pl.ds(2 * n0, 2 * R)], dst_ref=over.at[o],
+            send_sem=w_send.at[3], recv_sem=over_recv,
+            device_id={"tp": tp_at(to, c)}, device_id_type=MESH)
+
+    def over_out(group):
+        to = jnp.where(z == 1, 0, Z - 1)
+        for j, i in group:
+            for h in range(2):
+                pltpu.make_async_remote_copy(
+                    src_ref=piece(4, h, j, i), dst_ref=piece(3, h, j, i),
+                    send_sem=w_send.at[5], recv_sem=w_recv.at[3, h, j * X + i - 1],
+                    device_id={"tp": tp_at(to, c)}, device_id_type=MESH).start()
+
+    def tok_chain(direction, s, a):
         src = z - s if direction == 0 else z + s
         dst = z + 1 if direction == 0 else z - 1
         ok = jnp.logical_and(src >= 0, dst < Z) if direction == 0 else jnp.logical_and(src < Z, dst >= 0)
         src, dst = jnp.clip(src, 0, Z - 1), jnp.clip(dst, 0, Z - 1)
+        ref = nrm.at[c, src, pl.ds(a * strip, strip)]
         cp = pltpu.make_async_remote_copy(
-            src_ref=nrm.at[c, src], dst_ref=nrm.at[c, src],
-            send_sem=t_send.at[direction, s], recv_sem=t_recv.at[direction, s],
+            src_ref=ref, dst_ref=ref,
+            send_sem=t_send.at[direction], recv_sem=t_recv.at[direction, s, a],
             device_id={"tp": tp_at(dst, c)}, device_id_type=MESH)
         return cp, ok
 
-    def tok_sib(zz):
+    def tok_sib(zz, a):
+        ref = nrm.at[c, zz, pl.ds(a * strip, strip)]
         return pltpu.make_async_remote_copy(
-            src_ref=nrm.at[c, zz], dst_ref=nrm.at[c, zz],
-            send_sem=ts_send, recv_sem=ts_recv.at[zz],
+            src_ref=ref, dst_ref=ref,
+            send_sem=ts_send, recv_sem=ts_recv,
             device_id={"tp": tp_at(z, sib)}, device_id_type=MESH)
 
-    def tok_start(s):
-        for direction in range(2):
-            cp, ok = tok_chain(direction, s)
-            pl.when(ok)(cp.start)
-
-    def tok_arrive(s):
+    def tok_arrive(s, a):
         for direction in range(2):
             src = z - s if direction == 0 else z + s
             there = src >= 0 if direction == 0 else src < Z
@@ -146,37 +173,93 @@
 
             @pl.when(there)
             def _():
-                pltpu.make_async_copy(nrm.at[c, src], nrm.at[c, src], t_recv.at[direction, s - 1]).wait()
+                ref = nrm.at[c, src, pl.ds(a * strip, strip)]
+                pltpu.make_async_copy(ref, ref, t_recv.at[direction, s - 1, a]).wait()
                 if C > 1:
-                    tok_sib(src).start()
+                    tok_sib(src, a).start()
 
             if s < Z - 1:
-                cp, ok = tok_chain(direction, s)
+                cp, ok = tok_chain(direction, s, a)
                 pl.when(ok)(cp.start)
 
+    def over_relay():
+        for i in range(1, X):
+            w_wait(4, 0, 0, i)
+            for j in range(1, Y):
+                w_copy(4, 0, 0, i, j, 0)
+        for j in range(1, Y):
+            w_wait(4, 1, j, 0)
+            for i in range(1, X):
+                w_copy(4, 1, j, 0, 0, i)
+
+    def edge_direct():
+        for i in range(1, X):
+            w_wait(3, 0, 0, i)
+        for j in range(1, Y):
+            w_wait(3, 1, j, 0)
+
+    def over_cross():
+        wait_cross((4,))
+        over_out(in_row + in_col)
+
+    def over_diag():
+        wait_diag((4,))
+        over_out(far)
+
+    in_row = [(0, i) for i in range(1, X)]
+    in_col = [(j, 0) for j in range(1, Y)]
+    far = [(j, i) for j in range(1, Y) for i in range(1, X)]
+
     phase_one((0, 1))
-    values = tok_v[...].astype(F32)
-    factor = lax.rsqrt(jnp.mean(values * values, axis=-1, keepdims=True) + eps_floor)
-    nrm[c, z] = (values * factor * gain_v[...]).astype(BF16)
-    tok_start(0)
-    if C > 1:
-        tok_sib(z).start()
+    if R:
+        pl.when(edge)(lambda: over_in().start())
+    for a in range(strips):
+        part_rows = pl.ds(a * strip, strip)
+        values = tok_v[part_rows, :].astype(F32)
+        factor = lax.rsqrt(jnp.mean(values * values, axis=-1, keepdims=True) + eps_floor)
+        nrm[c, z, part_rows] = (values * factor * gain_v[...]).astype(BF16)
+        for direction in range(2):
+            cp, ok = tok_chain(direction, 0, a)
+            pl.when(ok)(cp.start)
+        if C > 1:
+            tok_sib(z, a).start()
+    if R:
+        @pl.when(inner)
+        def _():
+            pltpu.make_async_copy(over.at[f], over.at[f], over_recv).wait()
+            phase_one((4,))
+            phase_own((4,))
     phase_own((0, 1))
+    if R:
+        @pl.when(jnp.logical_not(edge))
+        def _():
+            phase_one((3,))
+            phase_own((3,))
     if Z > 1:
-        tok_arrive(1)
+        for a in range(strips):
+            tok_arrive(1, a)
+    if Z > 2:
+        tok_arrive(2, 0)
+    if R:
+        pl.when(inner)(over_relay)
     phase_relay((0, 1))
-    for s in range(2, Z):
-        tok_arrive(s)
-    wait_cross((0, 1))
+    if Z > 2:
+        for a in range(1, strips):
+            tok_arrive(2, a)
+    if R:
+        pl.when(inner)(over_cross)
+        pl.when(jnp.logical_not(edge))(lambda: phase_relay((3,)))
+    for s in range(3, Z):
+        for a in range(strips):
+            tok_arrive(s, a)
     phase_one((2,))
     phase_own((2,))
+    if R:
+        pl.when(inner)(over_diag)
     if C > 1:
-        for zz in range(Z):
-            ref = nrm.at[sib, zz]
-            pltpu.make_async_copy(ref, ref, ts_recv.at[zz]).wait()
+        pltpu.make_async_copy(nrm.at[sib], nrm.at[sib], ts_recv).wait()
 
     near = [(0, 0)] + [(0, i) for i in range(1, X)] + [(j, 0) for j in range(1, Y)]
-    far = [(j, i) for j in range(1, Y) for i in range(1, X)]
     mrows = tile * rows
     per_core = Z // tile
 
@@ -190,10 +273,11 @@
             total = p if total is None else total + p
         return total
 
+    wait_cross((0,))
+
     @pl.loop(0, C * per_core)
     def _(n):
         acc_g[n] = product(n, Wg, near)
-        acc_u[n] = product(n, Wu, near)
 
     wait_diag((0,))
 
@@ -204,7 +288,15 @@
             g = g + product(n, Wg, far)
         acc_g[n] = jax.nn.silu(g)
 
-    wait_diag((1,))
+    if R:
+        pl.when(edge)(edge_direct)
+    wait_cross(ups)
+
+    @pl.loop(0, C * per_core)
+    def _(n):
+        acc_u[n] = product(n, Wu, near)
+
+    wait_diag(ups)
 
     @pl.loop(0, C * per_core)
     def _(n):
@@ -325,16 +417,6 @@
                 far_low(q, k)
                 far_high(q, k)
 
-    def sum_last(qs):
-        for k in hops:
-            for q in qs:
-                if k + 1 < Z - 1:
-                    near_low(q, k + 1)
-                far_low(q, k)
-                far_high(q, k)
-                if k + 1 < Z - 1:
-                    near_high(q, k + 1)
-
     def sum_end(q):
         j, i, h = units[q]
         for direction, there in ((0, z > 0), (1, z < Z - 1)):
@@ -345,28 +427,26 @@
 
         out[:, pl.ds(pl.multiple_of((fs_at(j, i) * cuts + h) * N, N), N)] = part[q, z].astype(BF16)
 
-    in_row = [(0, i) for i in range(1, X)]
-    in_col = [(j, 0) for j in range(1, Y)]
     both = range(cuts)
     early = [(j, i, 0) for j, i in in_row] + [(j, i, 1) for j, i in in_col] if cuts == 2 else []
     mid = [(j, i, h) for h in both for j, i in in_row + in_col if (j, i, h) not in early]
     qa = down([(0, 0, h) for h in both], True)
+    sum_near(qa)
     phase_relay((2,))
     qb = down(early)
-    sum_near(qa)
+    sum_near(qb)
+    sum_far(qa)
     wait_cross((2,))
     qc = down(mid, hold=True)
-    sum_near(qb)
-    sum_far(qa)
+    sum_near(qc)
+    sum_far(qb)
     wait_diag((2,))
     qd = down([(j, i, h) for j, i in far for h in both], held=qc)
-    sum_near(qc)
-    sum_far(qb)
+    sum_near(qd)
+    sum_far(qc)
     for q in qa + qb:
         sum_end(q)
-    sum_far(qc)
-    sum_near(qd, range(min(1, Z - 1)))
-    sum_last(qd)
+    sum_far(qd)
     for q in qc + qd:
         sum_end(q)
 
@@ -374,12 +454,24 @@
         pltpu.make_async_copy(ref, ref, sem).wait()
 
     if F > 1:
-        for m in range(3):
-            sent(mats[m][1].at[pl.ds(0, F - 1)], w_send.at[m])
-    for s in range(Z - 1):
-        for direction in range(2):
-            cp, ok = tok_chain(direction, s)
-            pl.when(ok)(cp.wait_send)
+        most = pl.ds(0, F - 1)
+        sent(Wg.at[most], w_send.at[0])
+        sent(Wu.at[most, pl.ds(0, 2 * n0)], w_send.at[1])
+        sent(Wd.at[most], w_send.at[2])
+        if R:
+            pl.when(jnp.logical_not(edge))(lambda: sent(Wu.at[most, pl.ds(2 * n0, 2 * R)], w_send.at[3]))
+
+            @pl.when(inner)
+            def _():
+                sent(over.at[most], w_send.at[4])
+                sent(over.at[most], w_send.at[5])
+    if R:
+        pl.when(edge)(lambda: sent(over.at[f], w_send.at[3]))
+    for k in range(Z):
+        if k < Z - 1:
+            pl.when(z == k)(lambda: sent(nrm.at[c, pl.ds(0, k + 1)], t_send.at[0]))
+        if k > 0:
+            pl.when(z == k)(lambda: sent(nrm.at[c, pl.ds(k, Z - k)], t_send.at[1]))
     if C > 1:
         sent(nrm.at[c], ts_send)
         sent(sib_s, p_send)
@@ -397,11 +489,13 @@
     N = down_weight.shape[1] // cuts
     U = F * cuts
     tile = 2 if Z % 2 == 0 else 1
+    R = max(H * 3 // 44 // 16, 1) * 16 if Z >= 4 and F > 1 and H % 32 == 0 else 0
+    strips = 2 if rows % 32 == 0 else 1
     vmem = pl.BlockSpec(memory_space=pltpu.VMEM)
     dma = pltpu.SemaphoreType.DMA
     hbm = pl.BlockSpec(memory_space=pl.ANY)
     return pl.pallas_call(
-        functools.partial(kernel, Y, X, Z, C, cuts),
+        functools.partial(kernel, Y, X, Z, C, cuts, R),
         out_shape=pltpu.VMEM((rows, D), BF16),
         in_specs=[hbm] * 5,
         out_specs=vmem,
@@ -410,6 +504,7 @@
             pltpu.VMEM((F, H, K), BF16),
             pltpu.VMEM((F, H, K), BF16),
             pltpu.VMEM((F, H, N * cuts), BF16),
+            pltpu.VMEM((F, 2 * max(R, 8), K), BF16),
             pltpu.VMEM((C * Z // tile, tile * rows, H), F32),
             pltpu.VMEM((C * Z // tile, tile * rows, H), F32),
             pltpu.VMEM((C, Z, rows, H), BF16),
@@ -421,8 +516,8 @@
             pltpu.VMEM((rows, D), BF16),
             pltpu.VMEM((1, D), F32),
             dma((5,)),
-            dma((3,)), dma((3, 2, F)),
-            dma((2, max(Z - 1, 1))), dma((2, max(Z - 1, 1))), dma, dma((Z,)),
+            dma((6,)), dma((5, 2, max(F - 1, 1))), dma,
+            dma((2,)), dma((2, max(Z - 1, 1), strips)), dma, dma,
             dma, dma((U,)), dma, dma((U, Z + 1)),
         ],
         compiler_params=pltpu.CompilerParams(

time: 94.5 us -> 92.5 us (0.979)
  Pallas kernels: 93.6 us -> 91.6 us
    pallas_call x1, Pallas kernels: 93.6 us -> 91.6 us  [local(): pl.pallas_call(functools.partial(kernel, Y, X, Z, C, cuts, R), out_shape=...]
where the time goes in v3:
time: 92.5 us; the launch traced here: 92.4 us
  Pallas kernels  91.6 us (99%)
    pallas_call x1, Pallas kernels, local(): pl.pallas_call(functools.partial(kernel, Y, X, Z, C, cuts, R), out_shape=...  91.6 us

profile of v3, /device:TPU:0, one launch (start us, length us, event | category | flops | bytes accessed | tf_op | source)
XLA Modules:
  0.0 92.4 jit_solution(7971513012117699147)
XLA Ops:
  0.0 91.6 %shard_map.55 = bf16[128,2048]{1,0:T(8,128)(2,1)S(1)} custom-call(bf16[128,2048]{1,0:T(8,128)(2,1)} %tok.1, f32[1,2048]{1,0:T(1,128)} %bitcast.5, bf16[704,512]{1,0:T(8,128)(2,1)} %bitcast.3, bf16[704,512]{1,0:T(8,128)(2,1)} %bitcast.4, bf16[704,512]{1,0:T(8,128)(2,1)} %dw.1), custom_call_target="tpu_custom_call" | custom-call | tf_op jit(solution)/shard_map/pallas_call | solution.py:497
  91.6 0.8 copy.7

commit v4 on v3

--- a/solution.py
+++ b/solution.py
@@ -29,6 +29,8 @@
     strips = 2 if rows % 32 == 0 else 1
     strip = rows // strips
     ups = (1, 3) if R else (1,)
+    halves = (5, 6)
+    home = z // tile
     edge = jnp.logical_or(z == 0, z == Z - 1)
     inner = jnp.logical_or(z == 1, z == Z - 2)
 
@@ -74,15 +76,15 @@
             return Wu.at[o, pl.ds(2 * n0 + h * R, R)]
         if m == 4:
             return over.at[o, pl.ds(h * R, R)]
-        if cuts == 2:
-            return Wd.at[o, :, pl.ds(h * N, N)]
-        return Wd.at[o, pl.ds(h * (H // 2), H // 2)]
+        if m in (5, 6):
+            return Wd.at[o, pl.ds((m - 5) * (H // 2), H // 2), pl.ds(h * N, N)]
+        return Wd.at[o, :, pl.ds(h * N, N)]
 
     def w_copy(m, h, j, i, dj, di):
         slot = ((j - dj) % Y) * X + (i - di) % X
         cp = pltpu.make_async_remote_copy(
             src_ref=piece(m, h, j, i), dst_ref=piece(m, h, j, i),
-            send_sem=w_send.at[m], recv_sem=w_recv.at[m, h, slot - 1],
+            send_sem=w_send.at[2 if m in halves else m], recv_sem=w_recv.at[m, h, slot - 1],
             device_id={"fs": fs_at(dj, di)}, device_id_type=MESH)
         cp.start()
 
@@ -114,6 +116,27 @@
                 w_wait(m, 1, j, 0)
                 for i in range(1, X):
                     w_copy(m, 1, j, 0, 0, i)
+
+    def down_send(h):
+        for i in range(1, X):
+            w_copy(2, h, 0, 0, 0, i)
+        for j in range(1, Y):
+            w_copy(2, h, 0, 0, j, 0)
+
+    def down_relay(h):
+        for i in range(1, X):
+            w_wait(2, h, 0, i)
+            for j in range(1, Y):
+                w_copy(5, h, 0, i, j, 0)
+        for j in range(1, Y):
+            w_wait(2, h, j, 0)
+            for i in range(1, X):
+                w_copy(6, h, j, 0, 0, i)
+
+    def down_diag(h):
+        for j, i in far:
+            w_wait(5, h, j, i)
+            w_wait(6, h, j, i)
 
     def wait_cross(ms):
         for m in ms:
@@ -162,7 +185,7 @@
         ref = nrm.at[c, zz, pl.ds(a * strip, strip)]
         return pltpu.make_async_remote_copy(
             src_ref=ref, dst_ref=ref,
-            send_sem=ts_send, recv_sem=ts_recv,
+            send_sem=ts_send, recv_sem=ts_recv.at[jnp.where(zz // tile == home, 0, 1)],
             device_id={"tp": tp_at(z, sib)}, device_id_type=MESH)
 
     def tok_arrive(s, a):
@@ -209,6 +232,23 @@
     in_row = [(0, i) for i in range(1, X)]
     in_col = [(j, 0) for j in range(1, Y)]
     far = [(j, i) for j in range(1, Y) for i in range(1, X)]
+
+    near = [(0, 0)] + [(0, i) for i in range(1, X)] + [(j, 0) for j in range(1, Y)]
+    mrows = tile * rows
+    per_core = Z // tile
+
+    def product(n, held, group):
+        cc, zt = n // per_core, n % per_core
+        total = None
+        for j, i in group:
+            o = fs_at(j, i)
+            a = nrm[cc, pl.ds(zt * tile, tile), :, pl.ds(pl.multiple_of(o * K, K), K)].reshape(mrows, K)
+            p = lax.dot_general(a, held[o], (((1,), (1,)), ((), ())), preferred_element_type=F32)
+            total = p if total is None else total + p
+        return total
+
+    def gate_near(n):
+        acc_g[n] = product(n, Wg, near)
 
     phase_one((0, 1))
     if R:
@@ -249,35 +289,30 @@
     if R:
         pl.when(inner)(over_cross)
         pl.when(jnp.logical_not(edge))(lambda: phase_relay((3,)))
+    if C > 1:
+        ref = nrm.at[sib, pl.ds(home * tile, tile)]
+        pltpu.make_async_copy(ref, ref, ts_recv.at[0]).wait()
+    wait_cross((0,))
+
+    @pl.loop(0, C)
+    def _(cc):
+        gate_near(cc * per_core + home)
+
     for s in range(3, Z):
         for a in range(strips):
             tok_arrive(s, a)
-    phase_one((2,))
-    phase_own((2,))
+    for h in range(cuts):
+        down_send(h)
     if R:
         pl.when(inner)(over_diag)
-    if C > 1:
-        pltpu.make_async_copy(nrm.at[sib], nrm.at[sib], ts_recv).wait()
-
-    near = [(0, 0)] + [(0, i) for i in range(1, X)] + [(j, 0) for j in range(1, Y)]
-    mrows = tile * rows
-    per_core = Z // tile
-
-    def product(n, held, group):
-        cc, zt = n // per_core, n % per_core
-        total = None
-        for j, i in group:
-            o = fs_at(j, i)
-            a = nrm[cc, pl.ds(zt * tile, tile), :, pl.ds(pl.multiple_of(o * K, K), K)].reshape(mrows, K)
-            p = lax.dot_general(a, held[o], (((1,), (1,)), ((), ())), preferred_element_type=F32)
-            total = p if total is None else total + p
-        return total
-
-    wait_cross((0,))
-
-    @pl.loop(0, C * per_core)
-    def _(n):
-        acc_g[n] = product(n, Wg, near)
+    if C > 1 and per_core > 1:
+        ref = nrm.at[sib, pl.ds(0, Z - tile)]
+        pltpu.make_async_copy(ref, ref, ts_recv.at[1]).wait()
+
+    if per_core > 1:
+        @pl.loop(0, C * (per_core - 1))
+        def _(k):
+            gate_near(k // (per_core - 1) * per_core + lax.rem(home + 1 + k % (per_core - 1), per_core))
 
     wait_diag((0,))
 
@@ -308,37 +343,41 @@
     def sum_slot(direction, d, at):
         return d if direction == 0 else jnp.where(at == d, Z, d)
 
+    units = []
+
+    def spot(ref, q, *at):
+        return ref.at[(q, *at)]
+
     def sum_copy(q, direction, d):
         to = above if direction == 0 else below
         return pltpu.make_async_remote_copy(
-            src_ref=rs_s.at[q, d], dst_ref=rs_r.at[q, direction, d],
+            src_ref=spot(rs_s, q, d), dst_ref=spot(rs_r, q, direction, d),
             send_sem=q_send, recv_sem=q_recv.at[q, sum_slot(direction, d, to)],
             device_id={"tp": tp_at(to, c)}, device_id_type=MESH)
 
     def sum_wait(q, direction, d):
-        ref = rs_r.at[q, direction, d]
+        ref = spot(rs_r, q, direction, d)
         pltpu.make_async_copy(ref, ref, q_recv.at[q, sum_slot(direction, d, z)]).wait()
-
-    units = []
 
     def add_sib(q, d):
         if C > 1:
-            part[q, d] = part[q, d] + sib_r[q, d].astype(F32)
+            ref = spot(part, q, d)
+            ref[...] = ref[...] + spot(sib_r, q, d)[...].astype(F32)
 
     def open_sum(qs, direction, order):
         for d in order:
             for q in qs:
-                total = part[q, d]
+                total = spot(part, q, d)[...]
                 if C > 1:
-                    total = total + sib_r[q, d].astype(F32)
-                rs_s[q, d] = total.astype(BF16)
+                    total = total + spot(sib_r, q, d)[...].astype(F32)
+                spot(rs_s, q, d)[...] = total.astype(BF16)
                 sum_copy(q, direction, d).start()
 
     def settle(qs, hold, held):
         def ends(direction, order):
-            open_sum(qs, direction, order[:-1])
+            open_sum(qs, direction, order[:1])
             if not hold:
-                open_sum(held + qs, direction, order[-1:])
+                open_sum(held + qs, direction, order[1:])
 
         if Z > 1:
             pl.when(z == 0)(lambda: ends(0, list(range(Z - 1, 0, -1))))
@@ -355,23 +394,24 @@
         qs = list(range(len(units), len(units) + len(new)))
         units.extend(new)
 
-        def weight(q):
+        def times(of, q):
             j, i, h = units[q]
-            return Wd[fs_at(j, i), :, h * N:(h + 1) * N]
+            return jnp.dot(hid[of].reshape(Z * rows, H), Wd[fs_at(j, i), :, h * N:(h + 1) * N],
+                           preferred_element_type=F32)
 
         copies = []
         if C > 1:
             for q in qs:
-                sib_s[q] = jnp.dot(hid[sib].reshape(Z * rows, H), weight(q),
-                                   preferred_element_type=F32).astype(BF16).reshape(Z, rows, N)
+                ref = spot(sib_s, q, slice(None))
+                ref[...] = times(sib, q).astype(BF16).reshape(ref.shape)
                 cp = pltpu.make_async_remote_copy(
-                    src_ref=sib_s.at[q], dst_ref=sib_r.at[q], send_sem=p_send, recv_sem=p_recv.at[q],
+                    src_ref=ref, dst_ref=spot(sib_r, q, slice(None)), send_sem=p_send, recv_sem=p_recv.at[q],
                     device_id={"tp": tp_at(z, sib)}, device_id_type=MESH)
                 cp.start()
                 copies.append(cp)
         for k, q in enumerate(qs):
-            part[q] = jnp.dot(hid[c].reshape(Z * rows, H), weight(q),
-                              preferred_element_type=F32).reshape(Z, rows, N)
+            ref = spot(part, q, slice(None))
+            ref[...] = times(c, q).reshape(ref.shape)
             if C > 1:
                 copies[k].wait_recv()
             if apart:
@@ -386,7 +426,8 @@
         @pl.when(ok)
         def _():
             sum_wait(q, direction, d)
-            rs_s[q, d] = (part[q, d] + rs_r[q, direction, d].astype(F32)).astype(BF16)
+            total = spot(part, q, d)[...] + spot(rs_r, q, direction, d)[...].astype(F32)
+            spot(rs_s, q, d)[...] = total.astype(BF16)
             sum_copy(q, direction, d).start()
 
     def near_low(q, k):
@@ -419,36 +460,40 @@
 
     def sum_end(q):
         j, i, h = units[q]
+        mine = spot(part, q, z)
         for direction, there in ((0, z > 0), (1, z < Z - 1)):
             @pl.when(there)
             def _():
                 sum_wait(q, direction, z)
-                part[q, z] = part[q, z] + rs_r[q, direction, z].astype(F32)
-
-        out[:, pl.ds(pl.multiple_of((fs_at(j, i) * cuts + h) * N, N), N)] = part[q, z].astype(BF16)
+                mine[...] = mine[...] + spot(rs_r, q, direction, z)[...].astype(F32)
+
+        col = pl.multiple_of((fs_at(j, i) * cuts + h) * N, N)
+        out[:, pl.ds(col, N)] = mine[...].astype(BF16)
 
     both = range(cuts)
-    early = [(j, i, 0) for j, i in in_row] + [(j, i, 1) for j, i in in_col] if cuts == 2 else []
-    mid = [(j, i, h) for h in both for j, i in in_row + in_col if (j, i, h) not in early]
-    qa = down([(0, 0, h) for h in both], True)
-    sum_near(qa)
-    phase_relay((2,))
-    qb = down(early)
-    sum_near(qb)
-    sum_far(qa)
-    wait_cross((2,))
-    qc = down(mid, hold=True)
-    sum_near(qc)
-    sum_far(qb)
-    wait_diag((2,))
-    qd = down([(j, i, h) for j, i in far for h in both], held=qc)
-    sum_near(qd)
-    sum_far(qc)
-    for q in qa + qb:
-        sum_end(q)
-    sum_far(qd)
-    for q in qc + qd:
-        sum_end(q)
+    first, rest = hops[:1], hops[1:]
+    groups = [down([(0, 0, h) for h in both], True)]
+    sum_near(groups[0])
+    for h in both:
+        last = h == cuts - 1
+        down_relay(h)
+        groups.append(down([(j, i, h) for j, i in in_row + in_col], hold=last))
+        sum_near(groups[-1], first if last else hops)
+        sum_far(groups[-2])
+    tail = groups[-1:]
+    for h in both:
+        down_diag(h)
+        tail.append(down([(j, i, h) for j, i in far], hold=h < cuts - 1, held=sum(tail, [])))
+        sum_near(tail[-1], first)
+    for qs in groups[:-1]:
+        for q in qs:
+            sum_end(q)
+    for qs in tail:
+        sum_far(qs)
+        sum_near(qs, rest)
+    for qs in tail:
+        for q in qs:
+            sum_end(q)
 
     def sent(ref, sem):
         pltpu.make_async_copy(ref, ref, sem).wait()
@@ -516,8 +561,8 @@
             pltpu.VMEM((rows, D), BF16),
             pltpu.VMEM((1, D), F32),
             dma((5,)),
-            dma((6,)), dma((5, 2, max(F - 1, 1))), dma,
-            dma((2,)), dma((2, max(Z - 1, 1), strips)), dma, dma,
+            dma((6,)), dma((7, 2, max(F - 1, 1))), dma,
+            dma((2,)), dma((2, max(Z - 1, 1), strips)), dma, dma((2,)),
             dma, dma((U,)), dma, dma((U, Z + 1)),
         ],
         compiler_params=pltpu.CompilerParams(

time: 92.5 us -> 90.4 us (0.977)
  Pallas kernels: 91.6 us -> 89.4 us
    pallas_call x1, Pallas kernels: 91.6 us -> 89.4 us  [local(): pl.pallas_call(functools.partial(kernel, Y, X, Z, C, cuts, R), out_shape=...]
where the time goes in v4:
time: 90.4 us; the launch traced here: 90.2 us
  Pallas kernels  89.4 us (99%)
    pallas_call x1, Pallas kernels, local(): pl.pallas_call(functools.partial(kernel, Y, X, Z, C, cuts, R), out_shape=...  89.4 us

profile of v4, /device:TPU:0, one launch (start us, length us, event | category | flops | bytes accessed | tf_op | source)
XLA Modules:
  0.0 90.2 jit_solution(11260072028162507892)
XLA Ops:
  0.0 89.4 %shard_map.55 = bf16[128,2048]{1,0:T(8,128)(2,1)S(1)} custom-call(bf16[128,2048]{1,0:T(8,128)(2,1)} %tok.1, f32[1,2048]{1,0:T(1,128)} %bitcast.5, bf16[704,512]{1,0:T(8,128)(2,1)} %bitcast.3, bf16[704,512]{1,0:T(8,128)(2,1)} %bitcast.4, bf16[704,512]{1,0:T(8,128)(2,1)} %dw.1), custom_call_target="tpu_custom_call" | custom-call | tf_op jit(solution)/shard_map/pallas_call | solution.py:542
  89.4 0.8 copy.7

commit v5 on v4

--- a/solution.py
+++ b/solution.py
@@ -390,28 +390,31 @@
                 for q in qs:
                     add_sib(q, d)
 
+    def times(of, q, at=slice(None)):
+        j, i, h = units[q]
+        a = hid[of, at]
+        p = jnp.dot(a.reshape(-1, H), Wd[fs_at(j, i), :, h * N:(h + 1) * N], preferred_element_type=F32)
+        return p.reshape(*a.shape[:-1], N)
+
+    def pass_sib(q, sem, at=slice(None)):
+        ref = spot(sib_s, q, at)
+        ref[...] = times(sib, q, at).astype(BF16)
+        cp = pltpu.make_async_remote_copy(
+            src_ref=ref, dst_ref=spot(sib_r, q, at), send_sem=p_send, recv_sem=p_recv.at[sem],
+            device_id={"tp": tp_at(z, sib)}, device_id_type=MESH)
+        cp.start()
+        return cp
+
     def down(new, apart=False, hold=False, held=()):
         qs = list(range(len(units), len(units) + len(new)))
         units.extend(new)
 
-        def times(of, q):
-            j, i, h = units[q]
-            return jnp.dot(hid[of].reshape(Z * rows, H), Wd[fs_at(j, i), :, h * N:(h + 1) * N],
-                           preferred_element_type=F32)
-
         copies = []
         if C > 1:
-            for q in qs:
-                ref = spot(sib_s, q, slice(None))
-                ref[...] = times(sib, q).astype(BF16).reshape(ref.shape)
-                cp = pltpu.make_async_remote_copy(
-                    src_ref=ref, dst_ref=spot(sib_r, q, slice(None)), send_sem=p_send, recv_sem=p_recv.at[q],
-                    device_id={"tp": tp_at(z, sib)}, device_id_type=MESH)
-                cp.start()
-                copies.append(cp)
+            copies = [pass_sib(q, q) for q in qs]
         for k, q in enumerate(qs):
             ref = spot(part, q, slice(None))
-            ref[...] = times(c, q).reshape(ref.shape)
+            ref[...] = times(c, q)
             if C > 1:
                 copies[k].wait_recv()
             if apart:
@@ -457,6 +460,42 @@
             for q in qs:
                 far_low(q, k)
                 far_high(q, k)
+
+    def eager(new, sem, held=(), between=lambda: None):
+        if C == 1 or Z == 1:
+            q, = down([new], held=held)
+            sum_near([q], hops[:1])
+            return [q]
+        q = len(units)
+        units.append(new)
+        tip = jnp.where(low, Z - 1, 0)
+        others = pl.ds(jnp.where(low, 0, 1), Z - 1)
+        tip_in = pass_sib(q, q, tip)
+        spot(part, q, tip)[...] = times(c, q, tip)
+
+        def settle_tip():
+            tip_in.wait_recv()
+            pl.when(z == 0)(lambda: open_sum([q], 0, [Z - 1]))
+            pl.when(z == Z - 1)(lambda: open_sum([q], 1, [0]))
+            pl.when(jnp.logical_and(z > 0, z < Z - 1))(lambda: add_sib(q, tip))
+            near_low(q, 0)
+            near_high(q, 0)
+
+        pl.when(c == 0)(settle_tip)
+        others_in = pass_sib(q, sem, others)
+        pl.when(c > 0)(settle_tip)
+        between()
+        spot(part, q, others)[...] = times(c, q, others)
+        others_in.wait_recv()
+        pl.when(z == 0)(lambda: open_sum(list(held) + [q], 0, range(Z - 2, 0, -1)))
+        pl.when(z == Z - 1)(lambda: open_sum(list(held) + [q], 1, range(1, Z - 1)))
+
+        @pl.loop(0, Z)
+        def _(d):
+            @pl.when(jnp.logical_and(d != tip, jnp.logical_or(d == z, jnp.logical_and(z > 0, z < Z - 1))))
+            def _():
+                add_sib(q, d)
+        return [q]
 
     def sum_end(q):
         j, i, h = units[q]
@@ -472,8 +511,12 @@
 
     both = range(cuts)
     first, rest = hops[:1], hops[1:]
-    groups = [down([(0, 0, h) for h in both], True)]
-    sum_near(groups[0])
+    tail = []
+    qs = eager((0, 0, 0), F * cuts)
+    more = down([(0, 0, h) for h in both[1:]])
+    sum_near(more, first)
+    groups = [qs + more]
+    sum_near(groups[0], rest)
     for h in both:
         last = h == cuts - 1
         down_relay(h)
@@ -483,13 +526,18 @@
     tail = groups[-1:]
     for h in both:
         down_diag(h)
-        tail.append(down([(j, i, h) for j, i in far], hold=h < cuts - 1, held=sum(tail, [])))
-        sum_near(tail[-1], first)
+        new, held = [(j, i, h) for j, i in far], sum(tail, [])
+        if h == cuts - 1 and len(far) == 1:
+            tail.append(eager(new[0], F * cuts + 1, held, lambda: sum_far(tail[0])))
+        else:
+            tail.append(down(new, hold=h < cuts - 1, held=held))
+            sum_near(tail[-1], first)
     for qs in groups[:-1]:
         for q in qs:
             sum_end(q)
     for qs in tail:
-        sum_far(qs)
+        if qs is not tail[0] or len(far) != 1:
+            sum_far(qs)
         sum_near(qs, rest)
     for qs in tail:
         for q in qs:
@@ -563,7 +611,7 @@
             dma((5,)),
             dma((6,)), dma((7, 2, max(F - 1, 1))), dma,
             dma((2,)), dma((2, max(Z - 1, 1), strips)), dma, dma((2,)),
-            dma, dma((U,)), dma, dma((U, Z + 1)),
+            dma, dma((U + 2,)), dma, dma((U, Z + 1)),
         ],
         compiler_params=pltpu.CompilerParams(
             collective_id=0, has_side_effects=True, vmem_limit_bytes=60 * 1024 * 1024),

time: 90.4 us -> 89.7 us (level)
  no operation moved by 1% of the time
where the time goes in v5:
time: 89.7 us; the launch traced here: 89.6 us
  Pallas kernels  88.8 us (99%)
    pallas_call x1, Pallas kernels, local(): pl.pallas_call(functools.partial(kernel, Y, X, Z, C, cuts, R), out_shape=...  88.8 us

profile of v5, /device:TPU:0, one launch (start us, length us, event | category | flops | bytes accessed | tf_op | source)
XLA Modules:
  0.0 89.6 jit_solution(12799787422964361091)
XLA Ops:
  0.0 88.8 %shard_map.55 = bf16[128,2048]{1,0:T(8,128)(2,1)S(1)} custom-call(bf16[128,2048]{1,0:T(8,128)(2,1)} %tok.1, f32[1,2048]{1,0:T(1,128)} %bitcast.5, bf16[704,512]{1,0:T(8,128)(2,1)} %bitcast.3, bf16[704,512]{1,0:T(8,128)(2,1)} %bitcast.4, bf16[704,512]{1,0:T(8,128)(2,1)} %dw.1), custom_call_target="tpu_custom_call" | custom-call | tf_op jit(solution)/shard_map/pallas_call | solution.py:590
  88.8 0.8 copy.7
